TPU v7x, 32 devices: a whole 2x2x4 slice. The times are simulated.
32 devices in a mesh: sp: 8 (over z, y), tp: 4 (over x, core).
Axes of the slice: x: 2, y: 2, z: 4, core: 2. Of those that a mesh axis runs over, the one named last changes fastest.
Arguments:
- tokens: bfloat16 [8192, 4096], P('sp', 'tp'), may hold values from -16 to 16
- norm_gain: float32 [4096], replicated, may hold values from 0.1 to 1.9
- w_pool_in: bfloat16 [4096, 2048], P('sp', 'tp'), may hold values from -0.09375 to 0.09375
- w_query: bfloat16 [4096, 2048], P('sp', 'tp'), may hold values from -0.09375 to 0.09375
- w_key: bfloat16 [4096, 256], P('sp', 'tp'), may hold values from -0.09375 to 0.09375
- w_value: bfloat16 [4096, 256], P('sp', 'tp'), may hold values from -0.09375 to 0.09375
- pool_map: bfloat16 [4, 512, 512], P('tp'), may hold values from -0.25 to 0.25
- pool_scale: float32 [2048], P('tp'), may hold values from 0.3 to 3
- q_gain: float32 [64], replicated, may hold values from 0.1 to 1.9
- k_gain: float32 [64], replicated, may hold values from 0.1 to 1.9
- sinks: float32 [32], P('tp'), may hold values from 0 to 4
- w_out: bfloat16 [4096, 4096], P('tp', 'sp'), may hold values from -0.09375 to 0.09375
Outputs:
- layer_out: bfloat16 [8192, 4096], P(('sp', 'tp'))
All inputs are finite; a program needn't handle non-finite values.
Results may differ from a plain program's by a relative error of at most 0.012.
Values may be sent and summed in bfloat16 or wider, within the bound.
A program may use at most 128 MiB of HBM per device.

v0:
```python
import jax
import jax.numpy as jnp
from jax import lax
from jax.sharding import PartitionSpec as P

HEAD_DIM = 64
GROUP = 8
WINDOW = 128
GROUP_WIDTH = 512
Q_HEADS = 32
epsilon = 1e-06


def passed_along(value, axis, steps):
    count = lax.axis_size(axis)
    first, last = (max(0, -steps), min(count, count - steps))
    return lax.ppermute(value, axis, [(source, source + steps) for source in range(first, last)])


def rms_scale(values):
    return values * lax.rsqrt(jnp.mean(values * values, axis=-1, keepdims=True) + epsilon)


def local(
    tokens,
    norm_gain,
    w_pool_in,
    w_query,
    w_key,
    w_value,
    pool_map,
    pool_scale,
    q_gain,
    k_gain,
    sinks,
    w_out,
):
    tok_rows = tokens.shape[0]
    local_groups = w_key.shape[1] // HEAD_DIM
    seq_index = lax.axis_index("sp")
    group_first = lax.axis_index("tp") * local_groups
    gathered = lax.all_gather(tokens, "tp", axis=1, tiled=True)
    widened = gathered.astype(jnp.float32)
    normed = (rms_scale(widened) * norm_gain).astype(jnp.bfloat16)
    ext_rows = normed.shape[0]
    pieces = (
        lax.all_gather(w_pool_in, "sp", axis=0, tiled=True),
        lax.all_gather(w_query, "sp", axis=0, tiled=True),
        lax.all_gather(w_key, "sp", axis=0, tiled=True),
        lax.all_gather(w_value, "sp", axis=0, tiled=True),
    )
    pool_sum, query_sum, key_sum, value_sum = tuple(
        (
            jnp.dot(normed, weight_piece, preferred_element_type=jnp.float32)
            for weight_piece in pieces
        )
    )
    pool_in = pool_sum.astype(jnp.bfloat16)
    query_rows = lax.optimization_barrier(query_sum.astype(jnp.bfloat16))
    key_rows = lax.optimization_barrier(key_sum.astype(jnp.bfloat16))
    value_rows = value_sum.astype(jnp.bfloat16).reshape(ext_rows, local_groups, HEAD_DIM)
    query_float = query_rows.astype(jnp.float32).reshape(ext_rows, local_groups * GROUP, HEAD_DIM)
    query_normed = (
        (rms_scale(query_float) * q_gain)
        .astype(jnp.bfloat16)
        .reshape(ext_rows, local_groups, GROUP, HEAD_DIM)
    )
    key_float = key_rows.astype(jnp.float32).reshape(ext_rows, local_groups, HEAD_DIM)
    key_normed = (rms_scale(key_float) * k_gain).astype(jnp.bfloat16)
    key_width = local_groups * HEAD_DIM
    pair_tail = jnp.concatenate(
        [
            key_normed[tok_rows - WINDOW :].reshape(WINDOW, key_width),
            value_rows[tok_rows - WINDOW :].reshape(WINDOW, key_width),
        ],
        axis=1,
    )
    earlier_pairs, earlier_pool = passed_along((pair_tail, pool_in[tok_rows - 15 :]), "sp", 1)
    key_span = jnp.concatenate(
        [earlier_pairs[:, :key_width].reshape(WINDOW, local_groups, HEAD_DIM), key_normed], axis=0
    )
    value_span = jnp.concatenate(
        [earlier_pairs[:, key_width:].reshape(WINDOW, local_groups, HEAD_DIM), value_rows], axis=0
    )
    pool_span = jnp.concatenate([earlier_pool, pool_in], axis=0)
    positions = seq_index * tok_rows + jnp.arange(tok_rows, dtype=jnp.int32)
    group_ids = group_first + jnp.arange(local_groups, dtype=jnp.int32)
    spans = jnp.exp2((group_ids + 1).astype(jnp.float32))
    pool_float = pool_span.astype(jnp.float32).reshape(tok_rows + 15, local_groups, GROUP_WIDTH)
    sum_two = pool_float[1:] + pool_float[:-1]
    sum_four = sum_two[2:] + sum_two[:-2]
    sum_eight = sum_four[4:] + sum_four[:-4]
    sum_sixteen = sum_eight[8:] + sum_eight[:-8]
    span_pick = spans[None, :, None]
    running = jnp.where(
        span_pick < 3.0,
        sum_two[14 : 14 + tok_rows],
        jnp.where(
            span_pick < 6.0,
            sum_four[12 : 12 + tok_rows],
            jnp.where(span_pick < 12.0, sum_eight[8 : 8 + tok_rows], sum_sixteen),
        ),
    )
    counts = jnp.minimum(positions.astype(jnp.float32)[:, None] + 1.0, spans[None, :])
    pool_diff = (running / counts[:, :, None] - pool_float[15:]).astype(jnp.bfloat16)
    mapped = jnp.einsum("tlc,lcd->tld", pool_diff, pool_map, preferred_element_type=jnp.float32)
    pool_branch = rms_scale(mapped * pool_scale.reshape(local_groups, GROUP_WIDTH))
    blocks = tok_rows // WINDOW
    query_blocks = query_normed.reshape(blocks, WINDOW, local_groups, GROUP, HEAD_DIM)
    key_pairs = jnp.concatenate(
        [
            key_span[:tok_rows].reshape(blocks, WINDOW, local_groups, HEAD_DIM),
            key_span[WINDOW:].reshape(blocks, WINDOW, local_groups, HEAD_DIM),
        ],
        axis=1,
    )
    value_pairs = jnp.concatenate(
        [
            value_span[:tok_rows].reshape(blocks, WINDOW, local_groups, HEAD_DIM),
            value_span[WINDOW:].reshape(blocks, WINDOW, local_groups, HEAD_DIM),
        ],
        axis=1,
    )
    scores = jnp.einsum(
        "nqlgd,nkld->nlgqk", query_blocks, key_pairs, preferred_element_type=jnp.float32
    ) * HEAD_DIM ** (-0.5)
    query_pos = jnp.arange(WINDOW, dtype=jnp.int32)[:, None] + WINDOW
    key_pos = jnp.arange(2 * WINDOW, dtype=jnp.int32)[None, :]
    distance = query_pos - key_pos
    in_band = (distance >= 0) & (distance < WINDOW)
    key_global = (
        seq_index * tok_rows
        + jnp.arange(blocks, dtype=jnp.int32)[:, None] * WINDOW
        - WINDOW
        + jnp.arange(2 * WINDOW, dtype=jnp.int32)[None, :]
    )
    allowed = in_band[None] & (key_global >= 0)[:, None, :]
    head_ids = group_ids[:, None] * GROUP + jnp.arange(GROUP, dtype=jnp.int32)[None, :] + 1
    slopes = jnp.exp2(-8.0 * head_ids.astype(jnp.float32) / Q_HEADS)
    logits = (
        scores - slopes[None, :, :, None, None] * distance.astype(jnp.float32)[None, None, None]
    )
    exp_scores = jnp.exp(jnp.where(allowed[:, None, None], logits, -jnp.inf))
    sink_logits = sinks.reshape(local_groups, GROUP)
    denominator = jnp.sum(exp_scores, axis=-1) + jnp.exp(sink_logits)[None, :, :, None]
    weights_bf = (exp_scores / denominator[..., None]).astype(jnp.bfloat16)
    attended = jnp.einsum(
        "nlgqk,nkld->nqlgd", weights_bf, value_pairs, preferred_element_type=jnp.float32
    )
    attn_branch = rms_scale(attended.reshape(tok_rows, local_groups, GROUP_WIDTH))
    mixed_rows = (
        jnp.stack([pool_branch, attn_branch], axis=2)
        .reshape(tok_rows, 2 * local_groups * GROUP_WIDTH)
        .astype(jnp.bfloat16)
    )
    out_columns = lax.all_gather(w_out, "sp", axis=1, tiled=True)
    return lax.psum_scatter(
        jnp.dot(mixed_rows, out_columns, preferred_element_type=jnp.float32).astype(jnp.bfloat16),
        "tp",
        scatter_dimension=0,
        tiled=True,
    )


def solution(mesh):
    in_specs = (
        P("sp", "tp"),
        P(),
        P("sp", "tp"),
        P("sp", "tp"),
        P("sp", "tp"),
        P("sp", "tp"),
        P("tp", None, None),
        P("tp"),
        P(),
        P(),
        P("tp"),
        P("tp", "sp"),
    )
    out_specs = P(("sp", "tp"), None)
    return jax.shard_map(local, mesh=mesh, in_specs=in_specs, out_specs=out_specs, check_vma=False)
```

profile of v0, /device:TPU:0, one launch (start us, length us, event | category | flops | bytes accessed | tf_op | source)
XLA Modules:
  0.0 435.6 jit_solution(6995739875760048080)
XLA Ops:
  6.5 0.7 all-gather.5.cloned.1.call-update
  7.3 0.7 all-gather.7.cloned.1.call-update
  8.1 0.7 all-gather.9.cloned.1.call-update
  8.8 0.5 all-gather.11.cloned.1.call-update
  9.6 33.1 %all_gather.20 = bf16[4096,64]{0,1:T(8,128)(2,1)S(1)} all-gather(bf16[512,64]{0,1:T(8,128)(2,1)S(1)} %copy-done.7), channel_id=1, replica_groups=mesh['sp'=8,'tp'=4] {'sp'}, dimensions={0}, use_global_device_ids=true | all-gather | bytes 589824 | tf_op jit(solution)/shard_map/all_gather | solution.py:49
  42.7 31.2 %all_gather.21 = bf16[4096,64]{0,1:T(8,128)(2,1)S(1)} all-gather(bf16[512,64]{0,1:T(8,128)(2,1)S(1)} %copy-done.8), channel_id=1, replica_groups=mesh['sp'=8,'tp'=4] {'sp'}, dimensions={0}, use_global_device_ids=true | all-gather | bytes 589824 | tf_op jit(solution)/shard_map/all_gather | solution.py:50
  73.9 0.1 add_compare_fusion
  74.0 1.1 broadcast_multiply_fusion
  75.1 0.3 broadcast_and_fusion
  75.5 5.1 %fusion = f32[1024]{0:T(1024)S(1)} fusion(bf16[1024,4096]{1,0:T(8,128)(2,1)} %all-gather.5.cloned.1.call-done), kind=kLoop, calls=%fused_computation.2 | loop fusion | flops 12581888 | bytes 8392704 | tf_op jit(solution)/shard_map/reduce_sum | solution.py:21
  80.6 10.5 %fusion.2 = bf16[1024,4096]{1,0:T(8,128)(2,1)} fusion(bf16[1024,4096]{1,0:T(8,128)(2,1)} %all-gather.5.cloned.1.call-done, f32[4096]{0:T(1024)S(1)} %copy-done.9, f32[1024]{0:T(1024)S(1)} %add_rsqrt_fusion.2), kind=kLoop, calls=%fused_computation.4 | loop fusion | flops 16777216 | bytes 16797696 | tf_op jit(solution)/shard_map/convert_element_type | solution.py:44
  91.0 53.8 %all-gather.7.cloned.1.call-done = bf16[4096,512]{1,0:T(8,128)(2,1)} async-done(((bf16[512,512]{1,0:T(8,128)(2,1)}), bf16[4096,512]{1,0:T(8,128)(2,1)}) %all-gather.7.cloned.1.call-update) | async-done | bytes 4194320 | tf_op jit(solution)/shard_map/all_gather | solution.py:47
  144.9 9.2 %convolution_convert_fusion.2 = bf16[1024,512]{1,0:T(8,128)(2,1)S(1)} fusion(bf16[1024,4096]{1,0:T(8,128)(2,1)} %fusion.2, bf16[4096,512]{1,0:T(8,128)(2,1)} %all-gather.7.cloned.1.call-done), kind=kOutput, calls=%fused_computation.32 | convolution fusion | flops 4295491584 | bytes 13631488 | tf_op jit(solution)/shard_map/dot_general | solution.py:54
  154.1 2.8 collective-permute-start
  156.9 2.7 convolution_convert_fusion.4
  159.7 0.1 fusion.24
  159.8 2.7 convolution_convert_fusion.3
  162.4 4.0 collective-permute-start.1
  166.4 53.0 %all-gather.9.cloned.1.call-done = bf16[4096,512]{1,0:T(8,128)(2,1)} async-done(((bf16[512,512]{1,0:T(8,128)(2,1)}), bf16[4096,512]{1,0:T(8,128)(2,1)}) %all-gather.9.cloned.1.call-update) | async-done | bytes 4194320 | tf_op jit(solution)/shard_map/all_gather | solution.py:48
  219.4 10.0 %convolution_convert_fusion.1 = bf16[1024,512]{1,0:T(8,128)(2,1)} fusion(bf16[1024,4096]{1,0:T(8,128)(2,1)} %fusion.2, bf16[4096,512]{1,0:T(8,128)(2,1)} %all-gather.9.cloned.1.call-done), kind=kOutput, calls=%fused_computation.31 | convolution fusion | flops 4295491584 | bytes 13631488 | tf_op jit(solution)/shard_map/dot_general | solution.py:54
  229.4 1.5 copy.24
  230.9 2.9 convert_multiply_fusion.2
  233.8 2.9 copy.25
  236.7 1.8 bitcast_reduce_fusion
  238.6 0.5 copy.37
  239.1 0.1 fusion.49
  239.2 0.1 copy-done.12
  239.3 0.3 multiply_convert_fusion.1
  239.5 0.1 fusion.50
  239.8 0.7 copy-done.5
  240.5 0.3 maximum_convert_fusion
  240.8 0.3 slice_add_fusion.1
  241.1 0.3 slice_add_fusion
  241.4 0.3 slice_add_fusion.2
  241.7 0.4 copy-done.11
  242.1 1.4 multiply_reduce_fusion.1
  243.5 1.3 fusion.16
  244.9 2.5 fusion.5
  247.4 0.1 broadcast_add_fusion
  247.5 2.4 multiply_reduce_fusion
  249.9 2.5 copy.29
  252.4 1.7 reshape.363
  254.2 0.3 multiply_convert_fusion
  254.5 0.9 copy-done.3
  255.4 0.2 pad_maximum_fusion
  255.6 89.2 %all-gather.11.cloned.1.call-done = bf16[1024,4096]{1,0:T(8,128)(2,1)} async-done(((bf16[1024,512]{1,0:T(8,128)(2,1)}), bf16[1024,4096]{1,0:T(8,128)(2,1)}) %all-gather.11.cloned.1.call-update) | async-done | bytes 8388624 | tf_op jit(solution)/shard_map/all_gather | solution.py:156
  344.8 14.5 %convolution_convert_fusion = bf16[1024,4096]{1,0:T(8,128)(2,1)} fusion(bf16[1024,1024]{0,1:T(8,128)(2,1)S(1)} %bitcast.121, bf16[1024,4096]{1,0:T(8,128)(2,1)} %all-gather.11.cloned.1.call-done), kind=kOutput, calls=%fused_computation.9 | convolution fusion | flops 8594128896 | bytes 18874368 | tf_op jit(solution)/shard_map/dot_general | solution.py:158
  359.3 69.7 %reduce-scatter.2.cloned.1.call-done = bf16[256,4096]{1,0:T(8,128)(2,1)} async-done(((bf16[1024,4096]{1,0:T(8,128)(2,1)}), bf16[256,4096]{1,0:T(8,128)(2,1)}) %reduce-scatter.2.cloned.1.call-update) | async-done | bytes 2097168 | tf_op jit(solution)/shard_map/reduce_scatter | solution.py:157
  (59 shorter events, 0.6 us)
Async XLA Ops:
  6.5 235.2 %copy-start = (bf16[1,512,512]{2,1,0:T(8,128)(2,1)S(1)}, bf16[1,512,512]{2,1,0:T(8,128)(2,1)}, u32[]{:S(2)}) copy-start(bf16[1,512,512]{2,1,0:T(8,128)(2,1)} %param.18) | copy-start | bytes 1572868
  6.5 3.0 copy-start.7
  6.5 36.1 %copy-start.8 = (bf16[512,64]{0,1:T(8,128)(2,1)S(1)}, bf16[512,64]{0,1:T(8,128)(2,1)}, u32[]{:S(2)}) copy-start(bf16[512,64]{0,1:T(8,128)(2,1)} %param.17) | copy-start | bytes 196612
  6.5 68.9 %all-gather.5.cloned.1.call-start = ((), (), s32[]{:S(2)}) async-start(), calls=%async_computation.1 | async-start | bytes 10485760 | tf_op jit(solution)/shard_map/all_gather | solution.py:42
  7.3 66.7 %copy-start.13 = (f32[8]{0:T(128)S(1)}, f32[8]{0:T(128)}, u32[]{:S(2)}) copy-start(f32[8]{0:T(128)} %param.22) | copy-start | bytes 100
  7.3 137.6 %all-gather.7.cloned.1.call-start = ((), (), s32[]{:S(2)}) async-start(), calls=%async_computation.2 | async-start | bytes 4718592 | tf_op jit(solution)/shard_map/all_gather | solution.py:47
  8.0 211.4 %all-gather.9.cloned.1.call-start = ((), (), s32[]{:S(2)}) async-start(), calls=%async_computation.3 | async-start | bytes 4718592 | tf_op jit(solution)/shard_map/all_gather | solution.py:48
  8.8 336.1 %all-gather.11.cloned.1.call-start = ((), (), s32[]{:S(2)}) async-start(), calls=%async_computation.4 | async-start | bytes 9437184 | tf_op jit(solution)/shard_map/all_gather | solution.py:156
  9.3 419.7 %reduce-scatter.2.cloned.1.call-start = ((), (), s32[]{:S(2)}) async-start(), calls=%async_computation.5 | async-start | bytes 10485760 | tf_op jit(solution)/shard_map/reduce_scatter | solution.py:157
  75.4 5.1 %copy-start.9 = (f32[4096]{0:T(1024)S(1)}, f32[4096]{0:T(1024)}, u32[]{:S(2)}) copy-start(f32[4096]{0:T(1024)} %param.13) | copy-start | bytes 49156
  144.9 12.0 %copy-start.2 = (bf16[1024,4096]{1,0:T(8,128)(2,1)S(1)}, bf16[1024,4096]{1,0:T(8,128)(2,1)}, u32[]{:S(2)}) copy-start(bf16[1024,4096]{1,0:T(8,128)(2,1)} %fusion.2) | copy-start | bytes 25165828
  154.1 5.5 %copy-start.4 = (bf16[1024,512]{1,0:T(8,128)(2,1)}, bf16[1024,512]{1,0:T(8,128)(2,1)S(1)}, u32[]{:S(2)}) copy-start(bf16[1024,512]{1,0:T(8,128)(2,1)S(1)} %convolution_convert_fusion.2) | copy-start | bytes 3145732
  154.1 5.5 %copy-start.10 = (f32[64]{0:T(128)S(1)}, f32[64]{0:T(128)}, u32[]{:S(2)}) copy-start(f32[64]{0:T(128)} %param.21) | copy-start | bytes 772
  154.1 85.6 %collective-permute-start = (bf16[15,512]{1,0:T(8,128)(2,1)S(1)}, bf16[15,512]{1,0:T(8,128)(2,1)S(1)}, u32[]{:S(2)}, u32[]{:S(2)}) collective-permute-start(bf16[15,512]{1,0:T(8,128)(2,1)S(1)} %slice.86), channel_id=1, source_target_pairs={{0,4},{4,8},{8,12},{12,16},{16,20},{20,24},{24,28},{1,5},{5,9},{9,... | collective-permute-start | bytes 46088 | tf_op jit(solution)/shard_map/ppermute | solution.py:17
  162.4 82.3 %collective-permute-start.1 = (bf16[128,128]{0,1:T(8,128)(2,1)S(1)}, bf16[128,128]{0,1:T(8,128)(2,1)S(1)}, u32[]{:S(2)}, u32[]{:S(2)}) collective-permute-start(bf16[128,128]{0,1:T(8,128)(2,1)S(1)} %pad_maximum_fusion.3), channel_id=1, source_target_pairs={{0,4},{4,8},{8,12},{12,16},{16,20},{20,24},{24,28},{1,5},{5,9},{9,... | collective-permute-start | bytes 98312 | tf_op jit(solution)/shard_map/ppermute | solution.py:17
  238.6 0.7 copy-start.12
  239.3 1.2 copy-start.5
  241.4 0.7 copy-start.11
  243.5 1.4 copy-start.6
  254.2 1.2 copy-start.3
  359.3 69.8 %copy-start.1 = (bf16[1,512,512]{2,1,0:T(8,128)(2,1)S(1)}, bf16[1,512,512]{2,1,0:T(8,128)(2,1)}, u32[]{:S(2)}) copy-start(bf16[1,512,512]{2,1,0:T(8,128)(2,1)} %param.18) | copy-start | bytes 1572868
Sparse Core Ops, SparseCore 0:
  8.9 60.9 all-gather.4
  72.0 72.7 all-gather.6
  147.0 72.3 all-gather.8
  221.3 123.4 all-gather.10
  359.4 69.5 reduce-scatter.1
where the time goes:
time: 436 us
  waiting for transfers between devices  268 us (61%)
  blocking collectives  64.3 us (15%)
  matrix products  45.3 us (10%)
  other arithmetic  25.5 us (6%)
  between operations  13.6 us (3%)
  local copies, waits for them, and re-layouts  11.5 us (3%)
  starting transfers between devices  6.92 us (2%)
    all_gather x1, waiting for transfers between devices, local(): out_columns = lax.all_gather(w_out, 'sp', axis=1, tiled=True)  89.2 us
    reduce_scatter x1, waiting for transfers between devices, local(): lax.psum_scatter(jnp.dot(mixed_rows, out_columns, preferred_element_type=...  69.7 us
    all_gather x1, waiting for transfers between devices, local(): lax.all_gather(w_pool_in, 'sp', axis=0, tiled=True)  53.8 us
    all_gather x1, waiting for transfers between devices, local(): lax.all_gather(w_query, 'sp', axis=0, tiled=True)  53 us
    all_gather x1, blocking collectives, local(): lax.all_gather(w_key, 'sp', axis=0, tiled=True)  33.1 us
    all_gather x1, blocking collectives, local(): lax.all_gather(w_value, 'sp', axis=0, tiled=True)  31.2 us
    dot_general x4, matrix products, local(): jnp.dot(normed, weight_piece, preferred_element_type=jnp.float32)  24.5 us
    dot_general x1, matrix products, local(): jnp.dot(mixed_rows, out_columns, preferred_element_type=jnp.float32)  14.5 us
  transfers between devices with their start and end apart: 7, of which 4 were waited for; matrix products, arithmetic and copies ran while one was open for 15% of the time, Pallas kernels for 0%

commit v1 on v0

--- a/solution.py
+++ b/solution.py
@@ -1,3 +1,4 @@
+import functools
 import jax
 import jax.numpy as jnp
 from jax import lax
@@ -9,6 +10,26 @@
 GROUP_WIDTH = 512
 Q_HEADS = 32
 epsilon = 1e-06
+
+
+def cubes_return_all(arr, which_dim):
+    even = list(arr.shape[1:])
+    even[which_dim] *= arr.shape[0]
+    return jnp.moveaxis(arr, 0, which_dim).reshape(even)
+
+
+def frames_wrap(local_array, row_axis, row_dim):
+    many = lax.axis_size(row_axis)
+    pages = list(map(lambda dd: (dd, (dd + 1) % many), range(many)))
+    xs_all = [local_array]
+    while len(xs_all) < many:
+        xs_all.append(lax.ppermute(xs_all[-1], axis_name=row_axis, perm=pages))
+    b_next = lax.axis_index(row_axis)
+    xs_all = jnp.stack(xs_all)[(b_next - jnp.arange(many)) % many]
+    return cubes_return_all(xs_all, row_dim)
+
+
+apply_state_here = functools.partial(frames_wrap, row_axis="sp", row_dim=0)
 
 
 def passed_along(value, axis, steps):
@@ -45,7 +66,7 @@
     ext_rows = normed.shape[0]
     pieces = (
         lax.all_gather(w_pool_in, "sp", axis=0, tiled=True),
-        lax.all_gather(w_query, "sp", axis=0, tiled=True),
+        apply_state_here(w_query),
         lax.all_gather(w_key, "sp", axis=0, tiled=True),
         lax.all_gather(w_value, "sp", axis=0, tiled=True),
     )

time: 436 us -> 397 us (0.911)
  waiting for transfers between devices: 268 us -> 191 us
  blocking collectives: 64.3 us -> 92.3 us
  local copies, waits for them, and re-layouts: 11.5 us -> 25.1 us
  matrix products: 45.3 us -> 40.8 us
    ppermute x0 -> x7, waiting for transfers between devices: none -> 76.3 us  [frames_wrap(): xs_all.append(lax.ppermute(xs_all[-1], axis_name=row_axis, perm=pages))]
    all_gather x1, waiting for transfers between devices: 53.8 us -> 0.01 us  [local(): lax.all_gather(w_pool_in, 'sp', axis=0, tiled=True)]
    all_gather x1 -> x0, waiting for transfers between devices: 53 us -> none  [local(): lax.all_gather(w_query, 'sp', axis=0, tiled=True)]
    all_gather x1, waiting for transfers between devices: 89.2 us -> 44 us  [local(): out_columns = lax.all_gather(w_out, 'sp', axis=1, tiled=True)]
    all_gather x1, blocking collectives: 31.2 us -> 51.2 us  [local(): lax.all_gather(w_value, 'sp', axis=0, tiled=True)]
    all_gather x1, blocking collectives: 33.1 us -> 41.2 us  [local(): lax.all_gather(w_key, 'sp', axis=0, tiled=True)]
    unnamed x31 -> x40, local copies, waits for them, and re-layouts: 2.68 us -> 9.74 us
    gather x0 -> x1, local copies, waits for them, and re-layouts: none -> 4.94 us  [frames_wrap(): xs_all = jnp.stack(xs_all)[(b_next - jnp.arange(many)) % many]]
  transfers between devices with their start and end apart: 7 -> 13, of which waited for: 4 -> 7; matrix products, arithmetic and copies ran while one was open for 15% -> 19% of each run, Pallas kernels for 0% -> 0%
where the time goes in v1:
time: 397 us; the launch traced here: 396 us
  waiting for transfers between devices  191 us (48%)
  blocking collectives  92.3 us (23%)
  matrix products  40.8 us (10%)
  other arithmetic  26.8 us (7%)
  local copies, waits for them, and re-layouts  25.1 us (6%)
  between operations  13.7 us (3%)
  starting transfers between devices  6.19 us (2%)
    ppermute x7, waiting for transfers between devices, frames_wrap(): xs_all.append(lax.ppermute(xs_all[-1], axis_name=row_axis, perm=pages))  76.3 us
    reduce_scatter x1, waiting for transfers between devices, local(): lax.psum_scatter(jnp.dot(mixed_rows, out_columns, preferred_element_type=...  69.7 us
    all_gather x1, blocking collectives, local(): lax.all_gather(w_value, 'sp', axis=0, tiled=True)  51.2 us
    all_gather x1, waiting for transfers between devices, local(): out_columns = lax.all_gather(w_out, 'sp', axis=1, tiled=True)  44 us
    all_gather x1, blocking collectives, local(): lax.all_gather(w_key, 'sp', axis=0, tiled=True)  41.2 us
    dot_general x4, matrix products, local(): jnp.dot(normed, weight_piece, preferred_element_type=jnp.float32)  20 us
    dot_general x1, matrix products, local(): jnp.dot(mixed_rows, out_columns, preferred_element_type=jnp.float32)  14.5 us
    convert_element_type x1, other arithmetic, local(): normed = (rms_scale(widened) * norm_gain).astype(jnp.bfloat16)  10.4 us
  transfers between devices with their start and end apart: 13, of which 7 were waited for; matrix products, arithmetic and copies ran while one was open for 19% of the time, Pallas kernels for 0%

profile of v1, /device:TPU:0, one launch (start us, length us, event | category | flops | bytes accessed | tf_op | source)
XLA Modules:
  0.0 396.1 jit_solution(10496284695233939247)
XLA Ops:
  6.5 0.7 all-gather.4.cloned.1.call-update
  7.3 0.7 all-gather.6.cloned.1.call-update
  8.1 3.0 collective-permute-start.2
  11.3 15.0 %collective-permute-done.2 = bf16[512,512]{1,0:T(8,128)(2,1)S(1)} collective-permute-done((bf16[512,512]{1,0:T(8,128)(2,1)}, bf16[512,512]{1,0:T(8,128)(2,1)S(1)}, u32[]{:S(2)}, u32[]{:S(2)}) %collective-permute-start.2) | collective-permute-done | bytes 524320 | tf_op jit(solution)/shard_map/ppermute | solution.py:26
  26.4 15.7 %collective-permute-done.3 = bf16[512,512]{1,0:T(8,128)(2,1)S(1)} collective-permute-done((bf16[512,512]{1,0:T(8,128)(2,1)S(1)}, bf16[512,512]{1,0:T(8,128)(2,1)S(1)}, u32[]{:S(2)}, u32[]{:S(2)}) %collective-permute-start.3) | collective-permute-done | bytes 524320 | tf_op jit(solution)/shard_map/ppermute | solution.py:26
  42.1 41.2 %all_gather.17 = bf16[4096,64]{0,1:T(8,128)(2,1)S(1)} all-gather(bf16[512,64]{0,1:T(8,128)(2,1)} %param.16), channel_id=1, replica_groups=mesh['sp'=8,'tp'=4] {'sp'}, dimensions={0}, use_global_device_ids=true | all-gather | bytes 589824 | tf_op jit(solution)/shard_map/all_gather | solution.py:70
  83.3 0.7 copy-done.8
  84.1 51.2 %all_gather.18 = bf16[4096,64]{0,1:T(8,128)(2,1)S(1)} all-gather(bf16[512,64]{0,1:T(8,128)(2,1)S(1)} %copy-done.10), channel_id=1, replica_groups=mesh['sp'=8,'tp'=4] {'sp'}, dimensions={0}, use_global_device_ids=true | all-gather | bytes 589824 | tf_op jit(solution)/shard_map/all_gather | solution.py:71
  135.2 0.3 broadcast_and_fusion
  135.7 0.7 exp.8
  136.4 0.8 bitcast_dynamic-update-slice_fusion.7
  137.3 1.1 broadcast_multiply_fusion
  138.4 20.9 %collective-permute-done.6 = bf16[512,512]{1,0:T(8,128)(2,1)} collective-permute-done((bf16[512,512]{1,0:T(8,128)(2,1)}, bf16[512,512]{1,0:T(8,128)(2,1)}, u32[]{:S(2)}, u32[]{:S(2)}) %collective-permute-start.6) | collective-permute-done | bytes 524320 | tf_op jit(solution)/shard_map/ppermute | solution.py:26
  159.3 0.8 bitcast_dynamic-update-slice_fusion.6
  160.2 0.8 bitcast_dynamic-update-slice_fusion.5
  161.0 0.8 bitcast_dynamic-update-slice_fusion.4
  161.8 17.2 %collective-permute-done.7 = bf16[512,512]{1,0:T(8,128)(2,1)S(1)} collective-permute-done((bf16[512,512]{1,0:T(8,128)(2,1)}, bf16[512,512]{1,0:T(8,128)(2,1)S(1)}, u32[]{:S(2)}, u32[]{:S(2)}) %collective-permute-start.7) | collective-permute-done | bytes 524320 | tf_op jit(solution)/shard_map/ppermute | solution.py:26
  179.1 1.9 bitcast_dynamic-update-slice_fusion.3
  181.0 1.9 bitcast_dynamic-update-slice_fusion.2
  182.8 0.8 bitcast_dynamic-update-slice_fusion.1
  183.7 7.4 %collective-permute-done.8 = bf16[512,512]{1,0:T(8,128)(2,1)S(1)} collective-permute-done((bf16[512,512]{1,0:T(8,128)(2,1)S(1)}, bf16[512,512]{1,0:T(8,128)(2,1)S(1)}, u32[]{:S(2)}, u32[]{:S(2)}) %collective-permute-start.8) | collective-permute-done | bytes 524320 | tf_op jit(solution)/shard_map/ppermute | solution.py:26
  191.1 0.8 bitcast_dynamic-update-slice_fusion
  191.9 4.9 %gather_fusion = bf16[8,512,512]{2,1,0:T(8,128)(2,1)} fusion(bf16[8,512,512]{2,1,0:T(8,128)(2,1)} %bitcast_dynamic-update-slice_fusion, s32[1024]{0:T(1024)S(1)} %pad_clamp_fusion), kind=kCustom, calls=%fused_computation | custom fusion | bytes 8388640 | tf_op jit(solution)/shard_map/gather | solution.py:28
  196.8 5.1 %fusion = f32[1024]{0:T(1024)S(1)} fusion(bf16[1024,4096]{1,0:T(8,128)(2,1)} %all-gather.4.cloned.1.call-done), kind=kLoop, calls=%fused_computation.3 | loop fusion | flops 12581888 | bytes 8392704 | tf_op jit(solution)/shard_map/reduce_sum | solution.py:42
  201.9 10.4 %fusion.2 = bf16[1024,4096]{1,0:T(8,128)(2,1)} fusion(bf16[1024,4096]{1,0:T(8,128)(2,1)} %all-gather.4.cloned.1.call-done, f32[4096]{0:T(1024)S(1)} %copy-done.11, f32[1024]{0:T(1024)S(1)} %add_rsqrt_fusion.2), kind=kLoop, calls=%fused_computation.5 | loop fusion | flops 16777216 | bytes 16797696 | tf_op jit(solution)/shard_map/convert_element_type | solution.py:65
  212.4 9.2 %convolution_convert_fusion.2 = bf16[1024,512]{1,0:T(8,128)(2,1)S(1)} fusion(bf16[1024,4096]{1,0:T(8,128)(2,1)} %fusion.2, bf16[4096,512]{1,0:T(8,128)(2,1)} %all-gather.6.cloned.1.call-done), kind=kOutput, calls=%fused_computation.33 | convolution fusion | flops 4295491584 | bytes 13631488 | tf_op jit(solution)/shard_map/dot_general | solution.py:75
  221.7 1.6 collective-permute-start
  223.3 2.7 convolution_convert_fusion.4
  226.1 2.7 convolution_convert_fusion.3
  228.8 1.3 collective-permute-start.1
  230.1 5.5 %convolution_convert_fusion.1 = bf16[1024,512]{1,0:T(8,128)(2,1)} fusion(bf16[1024,4096]{1,0:T(8,128)(2,1)S(1)} %copy-done.2, bf16[4096,512]{1,0:T(8,128)(2,1)S(1)} %bitcast.140), kind=kOutput, calls=%fused_computation.32 | convolution fusion | flops 4295491584 | bytes 13631488 | tf_op jit(solution)/shard_map/dot_general | solution.py:75
  235.6 1.5 copy.24
  237.1 2.9 convert_multiply_fusion.2
  240.0 3.0 copy.25
  242.9 1.8 bitcast_reduce_fusion
  244.8 0.5 copy.37
  246.0 0.3 maximum_convert_fusion
  247.2 0.4 copy-done.13
  247.6 1.4 multiply_reduce_fusion.1
  249.0 1.3 fusion.16
  250.5 2.5 fusion.5
  253.0 2.4 multiply_reduce_fusion
  255.5 2.5 copy.29
  258.0 1.7 reshape.416
  260.0 1.4 pad_maximum_fusion
  261.4 44.0 %all-gather.8.cloned.1.call-done = bf16[1024,4096]{1,0:T(8,128)(2,1)} async-done(((bf16[1024,512]{1,0:T(8,128)(2,1)}), bf16[1024,4096]{1,0:T(8,128)(2,1)}) %all-gather.8.cloned.1.call-update) | async-done | bytes 8388624 | tf_op jit(solution)/shard_map/all_gather | solution.py:177
  305.4 14.5 %convolution_convert_fusion = bf16[1024,4096]{1,0:T(8,128)(2,1)} fusion(bf16[1024,1024]{0,1:T(8,128)(2,1)S(1)} %bitcast.141, bf16[1024,4096]{1,0:T(8,128)(2,1)} %all-gather.8.cloned.1.call-done), kind=kOutput, calls=%fused_computation.10 | convolution fusion | flops 8594128896 | bytes 18874368 | tf_op jit(solution)/shard_map/dot_general | solution.py:179
  319.9 69.7 %reduce-scatter.2.cloned.1.call-done = bf16[256,4096]{1,0:T(8,128)(2,1)} async-done(((bf16[1024,4096]{1,0:T(8,128)(2,1)}), bf16[256,4096]{1,0:T(8,128)(2,1)}) %reduce-scatter.2.cloned.1.call-update) | async-done | bytes 2097168 | tf_op jit(solution)/shard_map/reduce_scatter | solution.py:178
  (83 shorter events, 2.6 us)
Async XLA Ops:
  6.5 240.7 %copy-start = (bf16[1,512,512]{2,1,0:T(8,128)(2,1)S(1)}, bf16[1,512,512]{2,1,0:T(8,128)(2,1)}, u32[]{:S(2)}) copy-start(bf16[1,512,512]{2,1,0:T(8,128)(2,1)} %param.18) | copy-start | bytes 1572868
  6.5 129.9 %copy-start.7 = (bf16[512,512]{1,0:T(8,128)(2,1)S(1)}, bf16[512,512]{1,0:T(8,128)(2,1)}, u32[]{:S(2)}) copy-start(bf16[512,512]{1,0:T(8,128)(2,1)} %param.15) | copy-start | bytes 1572868
  6.5 77.5 %copy-start.10 = (bf16[512,64]{0,1:T(8,128)(2,1)S(1)}, bf16[512,64]{0,1:T(8,128)(2,1)}, u32[]{:S(2)}) copy-start(bf16[512,64]{0,1:T(8,128)(2,1)} %param.17) | copy-start | bytes 196612
  6.5 190.3 %all-gather.4.cloned.1.call-start = ((), (), s32[]{:S(2)}) async-start(), calls=%async_computation.1 | async-start | bytes 10485760 | tf_op jit(solution)/shard_map/all_gather | solution.py:63
  7.3 205.1 %all-gather.6.cloned.1.call-start = ((), (), s32[]{:S(2)}) async-start(), calls=%async_computation.2 | async-start | bytes 4718592 | tf_op jit(solution)/shard_map/all_gather | solution.py:68
  8.0 297.4 %all-gather.8.cloned.1.call-start = ((), (), s32[]{:S(2)}) async-start(), calls=%async_computation.3 | async-start | bytes 9437184 | tf_op jit(solution)/shard_map/all_gather | solution.py:177
  8.1 18.2 %collective-permute-start.2 = (bf16[512,512]{1,0:T(8,128)(2,1)}, bf16[512,512]{1,0:T(8,128)(2,1)S(1)}, u32[]{:S(2)}, u32[]{:S(2)}) collective-permute-start(bf16[512,512]{1,0:T(8,128)(2,1)} %param.15), channel_id=1, source_target_pairs={{0,4},{4,8},{8,12},{12,16},{16,20},{20,24},{24,28},{28,0},{1,5},{5... | collective-permute-start | bytes 1572872 | tf_op jit(solution)/shard_map/ppermute | solution.py:26
  11.1 378.5 %reduce-scatter.2.cloned.1.call-start = ((), (), s32[]{:S(2)}) async-start(), calls=%async_computation.4 | async-start | bytes 10485760 | tf_op jit(solution)/shard_map/reduce_scatter | solution.py:178
  26.3 15.8 %collective-permute-start.3 = (bf16[512,512]{1,0:T(8,128)(2,1)S(1)}, bf16[512,512]{1,0:T(8,128)(2,1)S(1)}, u32[]{:S(2)}, u32[]{:S(2)}) collective-permute-start(bf16[512,512]{1,0:T(8,128)(2,1)S(1)} %collective-permute-done.2), channel_id=1, source_target_pairs={{0,4},{4,8},{8,12},{12,16},{16,20},{20,24},{24,28},{28,0},{1,5},{5... | collective-permute-start | bytes 1572872 | tf_op jit(solution)/shard_map/ppermute | solution.py:26
  42.1 41.2 %collective-permute-start.4 = (bf16[512,512]{1,0:T(8,128)(2,1)S(1)}, bf16[512,512]{1,0:T(8,128)(2,1)S(1)}, u32[]{:S(2)}, u32[]{:S(2)}) collective-permute-start(bf16[512,512]{1,0:T(8,128)(2,1)S(1)} %collective-permute-done.3), channel_id=1, source_target_pairs={{0,4},{4,8},{8,12},{12,16},{16,20},{20,24},{24,28},{28,0},{1,5},{5... | collective-permute-start | bytes 1572872 | tf_op jit(solution)/shard_map/ppermute | solution.py:26
  83.3 0.8 copy-start.8
  83.3 52.3 %collective-permute-start.5 = (bf16[512,512]{1,0:T(8,128)(2,1)S(1)}, bf16[512,512]{1,0:T(8,128)(2,1)}, u32[]{:S(2)}, u32[]{:S(2)}) collective-permute-start(bf16[512,512]{1,0:T(8,128)(2,1)S(1)} %collective-permute-done.4), channel_id=1, source_target_pairs={{0,4},{4,8},{8,12},{12,16},{16,20},{20,24},{24,28},{28,0},{1,5},{5... | collective-permute-start | bytes 1572872 | tf_op jit(solution)/shard_map/ppermute | solution.py:26
  135.6 23.7 %collective-permute-start.6 = (bf16[512,512]{1,0:T(8,128)(2,1)}, bf16[512,512]{1,0:T(8,128)(2,1)}, u32[]{:S(2)}, u32[]{:S(2)}) collective-permute-start(bf16[512,512]{1,0:T(8,128)(2,1)} %collective-permute-done.5), channel_id=1, source_target_pairs={{0,4},{4,8},{8,12},{12,16},{16,20},{20,24},{24,28},{28,0},{1,5},{5... | collective-permute-start | bytes 1572872 | tf_op jit(solution)/shard_map/ppermute | solution.py:26
  135.7 25.3 %copy-start.9 = (bf16[512,512]{1,0:T(8,128)(2,1)S(1)}, bf16[512,512]{1,0:T(8,128)(2,1)}, u32[]{:S(2)}) copy-start(bf16[512,512]{1,0:T(8,128)(2,1)} %copy-done.8) | copy-start | bytes 1572868
  159.3 19.8 %collective-permute-start.7 = (bf16[512,512]{1,0:T(8,128)(2,1)}, bf16[512,512]{1,0:T(8,128)(2,1)S(1)}, u32[]{:S(2)}, u32[]{:S(2)}) collective-permute-start(bf16[512,512]{1,0:T(8,128)(2,1)} %collective-permute-done.6), channel_id=1, source_target_pairs={{0,4},{4,8},{8,12},{12,16},{16,20},{20,24},{24,28},{28,0},{1,5},{5... | collective-permute-start | bytes 1572872 | tf_op jit(solution)/shard_map/ppermute | solution.py:26
  179.1 12.0 %collective-permute-start.8 = (bf16[512,512]{1,0:T(8,128)(2,1)S(1)}, bf16[512,512]{1,0:T(8,128)(2,1)S(1)}, u32[]{:S(2)}, u32[]{:S(2)}) collective-permute-start(bf16[512,512]{1,0:T(8,128)(2,1)S(1)} %collective-permute-done.7), channel_id=1, source_target_pairs={{0,4},{4,8},{8,12},{12,16},{16,20},{20,24},{24,28},{28,0},{1,5},{5... | collective-permute-start | bytes 1572872 | tf_op jit(solution)/shard_map/ppermute | solution.py:26
  196.8 5.1 %copy-start.11 = (f32[4096]{0:T(1024)S(1)}, f32[4096]{0:T(1024)}, u32[]{:S(2)}) copy-start(f32[4096]{0:T(1024)} %param.13) | copy-start | bytes 49156
  212.4 10.9 %copy-start.2 = (bf16[1024,4096]{1,0:T(8,128)(2,1)S(1)}, bf16[1024,4096]{1,0:T(8,128)(2,1)}, u32[]{:S(2)}) copy-start(bf16[1024,4096]{1,0:T(8,128)(2,1)} %fusion.2) | copy-start | bytes 25165828
  221.6 4.3 %copy-start.4 = (bf16[1024,512]{1,0:T(8,128)(2,1)}, bf16[1024,512]{1,0:T(8,128)(2,1)S(1)}, u32[]{:S(2)}) copy-start(bf16[1024,512]{1,0:T(8,128)(2,1)S(1)} %convolution_convert_fusion.2) | copy-start | bytes 3145732
  221.6 4.4 %copy-start.12 = (f32[64]{0:T(128)S(1)}, f32[64]{0:T(128)}, u32[]{:S(2)}) copy-start(f32[64]{0:T(128)} %param.21) | copy-start | bytes 772
  221.7 24.2 %collective-permute-start = (bf16[15,512]{1,0:T(8,128)(2,1)S(1)}, bf16[15,512]{1,0:T(8,128)(2,1)S(1)}, u32[]{:S(2)}, u32[]{:S(2)}) collective-permute-start(bf16[15,512]{1,0:T(8,128)(2,1)S(1)} %slice.88), channel_id=1, source_target_pairs={{0,4},{4,8},{8,12},{12,16},{16,20},{20,24},{24,28},{1,5},{5,9},{9,... | collective-permute-start | bytes 46088 | tf_op jit(solution)/shard_map/ppermute | solution.py:38
  226.1 4.0 %copy-start.3 = (bf16[8,512,512]{2,1,0:T(8,128)(2,1)S(1)}, bf16[8,512,512]{2,1,0:T(8,128)(2,1)}, u32[]{:S(2)}) copy-start(bf16[8,512,512]{2,1,0:T(8,128)(2,1)} %gather_fusion) | copy-start | bytes 12582916
  228.8 21.6 %collective-permute-start.1 = (bf16[128,128]{0,1:T(8,128)(2,1)S(1)}, bf16[128,128]{0,1:T(8,128)(2,1)S(1)}, u32[]{:S(2)}, u32[]{:S(2)}) collective-permute-start(bf16[128,128]{0,1:T(8,128)(2,1)S(1)} %pad_maximum_fusion.3), channel_id=1, source_target_pairs={{0,4},{4,8},{8,12},{12,16},{16,20},{20,24},{24,28},{1,5},{5,9},{9,... | collective-permute-start | bytes 98312 | tf_op jit(solution)/shard_map/ppermute | solution.py:38
  242.9 2.5 copy-start.14
  244.8 1.2 copy-start.5
  246.9 0.7 copy-start.13
  249.0 1.4 copy-start.6
  319.9 69.7 %copy-start.1 = (bf16[1,512,512]{2,1,0:T(8,128)(2,1)S(1)}, bf16[1,512,512]{2,1,0:T(8,128)(2,1)}, u32[]{:S(2)}) copy-start(bf16[1,512,512]{2,1,0:T(8,128)(2,1)} %param.18) | copy-start | bytes 1572868
Sparse Core Ops, SparseCore 0:
  8.9 60.9 all-gather.3
  72.0 97.2 all-gather.5
  171.3 134.0 all-gather.7
  320.0 69.5 reduce-scatter.1
